TPU v7x, 32 devices: a whole 2x2x4 slice. The times are simulated.
32 devices in a mesh: sp: 16 (over z, y, x), tp: 2 (over core).
Axes of the slice: x: 2, y: 2, z: 4, core: 2. Of those that a mesh axis runs over, the one named last changes fastest.
Arguments:
- queries: bfloat16 [8192, 1024], P('sp', 'tp'), may hold values from -8 to 8
- key_rows: bfloat16 [8192, 512], P('sp', 'tp'), may hold values from -8 to 8
- values: bfloat16 [8192, 512], P('sp', 'tp'), may hold values from -16 to 16
- doc_ids: int32 [8192], P('sp'), may hold values from 0 to 7, never falling along the last dimension, each value on 1 to 2048 neighbouring positions
- sink_logits: float32 [16], P('tp'), may hold values from 2.5 to 6
- residual: bfloat16 [8192, 2048], P('sp'), may hold values from -6 to 6
- out_weight: bfloat16 [1024, 2048], P('tp'), may hold values from -0.1875 to 0.1875
- norm_gain: float32 [2048], replicated, may hold values from 0.1 to 1.9
- w_gate: bfloat16 [2048, 5632], P('sp', 'tp'), may hold values from -0.125 to 0.125
- w_up: bfloat16 [2048, 5632], P('sp', 'tp'), may hold values from -0.125 to 0.125
- w_down: bfloat16 [5632, 2048], P('tp', 'sp'), may hold values from -0.078125 to 0.078125
Outputs:
- layer_out: bfloat16 [8192, 2048], P('sp')
Inputs may be any that keep to these rules, and one draw needn't show every extreme that they name: `doc_ids`: document numbers never fall along the positions; each document has 1 to 2048 positions.
All inputs are finite; a program needn't handle non-finite values.
Results may differ from a plain program's by a relative error of at most 0.014.
Values may be sent and summed in bfloat16 or wider, within the bound.
A program may use at most 128 MiB of HBM per device.

v0:
```python
import jax
import jax.numpy as jnp
from jax import lax
from jax.sharding import PartitionSpec as P


HD = 64
WINDOW = 128
INNER = 4
CHUNKS = 2


def from_behind(shard, axis, by):
    size = lax.axis_size(axis)
    pairs = [(i, i + by) for i in range(size) if 0 <= i + by < size]
    return lax.ppermute(shard, axis, pairs)


def rms_norm(stream, norm_gain):
    floats = stream.astype(jnp.float32)
    scale = lax.rsqrt(jnp.mean(floats * floats, axis=-1, keepdims=True) + 1e-06)
    return floats * scale * norm_gain


def band_rows(tensor, blocks):
    tensor = tensor.reshape((blocks + 1, WINDOW) + tensor.shape[1:])
    return jnp.concatenate([tensor[:-1], tensor[1:]], axis=1)


def attend(queries, key_rows, values, doc_ids, sink_logits):
    local_rows = queries.shape[0]
    blocks = local_rows // WINDOW
    kv_local = key_rows.shape[1] // HD
    per_kv = queries.shape[1] // key_rows.shape[1]
    tail_docs = doc_ids[local_rows - WINDOW :] + 1
    width = key_rows.shape[1]
    tail = jnp.concatenate(
        [
            key_rows[local_rows - WINDOW :],
            values[local_rows - WINDOW :],
            jnp.broadcast_to(tail_docs.astype(jnp.bfloat16)[:, None], (WINDOW, 128)),
        ],
        axis=1,
    )
    tail = from_behind(tail, "sp", 1)
    prev_keys, prev_values = tail[:, :width], tail[:, width : 2 * width]
    prev_docs = tail[:, 2 * width].astype(jnp.int32)
    key_band = band_rows(jnp.concatenate([prev_keys, key_rows], axis=0), blocks).reshape(
        blocks, 2 * WINDOW, kv_local, HD
    )
    value_band = band_rows(jnp.concatenate([prev_values, values], axis=0), blocks).reshape(
        blocks, 2 * WINDOW, kv_local, HD
    )
    doc_band = band_rows(jnp.concatenate([prev_docs - 1, doc_ids]), blocks)
    query_band = queries.reshape(blocks, WINDOW, kv_local, per_kv, HD)
    scores = jnp.einsum(
        "nqhgd,nkhd->nhgqk", query_band, key_band, preferred_element_type=jnp.float32
    ) * HD ** (-0.5)
    offsets = jnp.arange(WINDOW)[:, None] + WINDOW - jnp.arange(2 * WINDOW)[None, :]
    inside = (offsets >= 0) & (offsets < WINDOW)
    query_docs = doc_ids.reshape(blocks, WINDOW)
    allowed = inside[None] & (query_docs[:, :, None] == doc_band[:, None, :])
    scores = jnp.where(allowed[:, None, None], scores, -1e30)
    sink_logit = sink_logits.reshape(kv_local, per_kv)[None, :, :, None, None]
    peak = jnp.maximum(jnp.max(scores, axis=-1, keepdims=True), sink_logit)
    raised = jnp.exp(scores - peak)
    denom = jnp.sum(raised, axis=-1, keepdims=True) + jnp.exp(sink_logit - peak)
    weights = (raised / denom).astype(jnp.bfloat16)
    attended = jnp.einsum(
        "nhgqk,nkhd->nqhgd", weights, value_band, preferred_element_type=jnp.float32
    )
    return attended.astype(jnp.bfloat16).reshape(local_rows, queries.shape[1])


def swap(shard, axis, by):
    size = lax.axis_size(axis)
    return lax.ppermute(shard, axis, [(i, i ^ by) for i in range(size)])


def piece_of(tensor, index, axis, pieces):
    size = tensor.shape[axis] // pieces
    return lax.dynamic_slice_in_dim(tensor, index * size, size, axis)


def in_order(mine, others, place, axis):
    size = mine.shape[axis]
    shape = list(mine.shape)
    shape[axis] = size * (len(others) + 1)
    whole = jnp.zeros(shape, mine.dtype)
    for k, shard in enumerate([mine] + others):
        whole = lax.dynamic_update_slice_in_dim(whole, shard, (place ^ k) * size, axis)
    return whole


def on_device(
    queries,
    key_rows,
    values,
    doc_ids,
    sink_logits,
    residual,
    out_weight,
    norm_gain,
    w_gate,
    w_up,
    w_down,
):
    inner = INNER
    outer = lax.axis_size("sp") // inner
    tp = lax.axis_size("tp")
    seat = lax.rem(lax.axis_index("sp"), inner)
    core = lax.axis_index("tp")
    columns = [[row + inner * step for step in range(outer)] for row in range(inner)]

    def gate_up_piece(k):
        return jnp.concatenate(
            [piece_of(w_gate, seat ^ k, 1, inner), piece_of(w_up, seat ^ k, 1, inner)], axis=1
        )

    def down_piece(k):
        return piece_of(w_down, seat ^ k, 0, inner)[None]

    gate_up_pieces = [gate_up_piece(k) for k in range(inner)]
    gate_up_pieces, queries, key_rows, values, w_down = lax.optimization_barrier(
        (gate_up_pieces, queries, key_rows, values, w_down)
    )
    gate_up = in_order(
        gate_up_pieces[0], [swap(gate_up_pieces[k], "sp", k) for k in range(1, inner)], seat, 0
    )
    down = in_order(
        down_piece(0), [swap(down_piece(k), "sp", k) for k in range(1, inner)], seat, 0
    )

    def across(block):
        return lax.all_gather(block, "sp", axis=0, tiled=True, axis_index_groups=columns)

    def flat(gathered):
        return jnp.swapaxes(gathered, 0, 1).reshape(gathered.shape[1], -1)

    part = inner // CHUNKS
    gate_up = across(gate_up)
    downs = []
    for c in range(CHUNKS):
        downs.append(across(down[c * part : (c + 1) * part]))

    attended = attend(queries, key_rows, values, doc_ids, sink_logits)
    mix_term = jnp.dot(attended, out_weight, preferred_element_type=jnp.float32).astype(jnp.bfloat16)
    mixed_sum = piece_of(mix_term, core, 0, tp).astype(jnp.float32)
    for k in range(1, tp):
        mixed_sum += swap(piece_of(mix_term, core ^ k, 0, tp), "tp", k).astype(jnp.float32)
    stream = (piece_of(residual, core, 0, tp).astype(jnp.float32) + mixed_sum).astype(jnp.bfloat16)
    normed = rms_norm(stream, norm_gain).astype(jnp.bfloat16)
    rows, width = normed.shape
    near = jnp.concatenate([normed] + [swap(normed, "sp", k) for k in range(1, inner)], axis=0)
    tokens = jnp.concatenate([near] + [swap(near, "tp", k) for k in range(1, tp)], axis=0)

    acts = jnp.dot(tokens, gate_up, preferred_element_type=jnp.float32)
    units = acts.shape[1] // 2
    hidden = (jax.nn.silu(acts[:, :units]) * acts[:, units:]).astype(jnp.bfloat16)
    block = width // (outer * CHUNKS)
    outs = []
    for c in range(CHUNKS):
        mlp_term = jnp.dot(hidden, lax.optimization_barrier(flat(downs[c])), preferred_element_type=jnp.float32)
        mlp_term = mlp_term.astype(jnp.bfloat16).reshape(tp, inner * rows, width // CHUNKS)
        near_sum = mlp_term[0].astype(jnp.float32)
        for k in range(1, tp):
            near_sum += swap(mlp_term[k], "tp", k).astype(jnp.float32)
        near_sum = near_sum.reshape(inner, rows, width // CHUNKS)
        sends = [near_sum[k].astype(jnp.bfloat16) for k in range(1, inner)]
        total = near_sum[0]
        for k in range(1, inner):
            sent = swap(sends[k - 1], "sp", k)
            total += sent.astype(jnp.float32)
        outs.append(total)
    total = jnp.concatenate(
        [outs[c][:, o * block : (o + 1) * block] for o in range(outer) for c in range(CHUNKS)],
        axis=1,
    )
    out = (stream.astype(jnp.float32) + total).astype(jnp.bfloat16)
    return in_order(out, [swap(out, "tp", k) for k in range(1, tp)], core, 0)


def solution(mesh):
    in_specs = (
        P("sp", "tp"),
        P("sp", "tp"),
        P("sp", "tp"),
        P("sp"),
        P("tp"),
        P("sp", None),
        P("tp", None),
        P(),
        P("sp", "tp"),
        P("sp", "tp"),
        P("tp", "sp"),
    )
    out_specs = P("sp", None)

    return jax.shard_map(
        on_device, mesh=mesh, in_specs=in_specs, out_specs=out_specs, check_vma=False
    )
```

profile of v0, /device:TPU:0, one launch (start us, length us, event | category | flops | bytes accessed | tf_op | source)
XLA Modules:
  0.0 299.2 jit_solution(16407825231187268255)
XLA Ops:
  6.5 2.4 constant_dynamic-slice_fusion.1
  13.3 5.5 %collective-permute-start = (bf16[128,640]{1,0:T(8,128)(2,1)}, bf16[128,640]{1,0:T(8,128)(2,1)}, u32[]{:S(2)}, u32[]{:S(2)}) collective-permute-start(bf16[128,640]{1,0:T(8,128)(2,1)} %pad_maximum_fusion.7), channel_id=1, source_target_pairs={{0,2},{2,4},{4,6},{6,8},{8,10},{10,12},{12,14},{14,16},{16,18},{18... | collective-permute-start | bytes 491528 | tf_op jit(solution)/shard_map/ppermute | solution.py:16
  25.8 2.0 reshape.139
  27.8 2.0 reshape.137
  29.8 3.5 %reshape.140 = bf16[4,128,4,2,64]{4,3,2,1,0:T(2,128)(2,1)} reshape(bf16[512,512]{1,0:T(8,128)(2,1)} %param.11) | data formatting | bytes 1048576 | tf_op jit(solution)/shard_map/reshape | solution.py:55
  35.9 1.9 copy.51
  45.6 2.1 collective-permute-done.10
  47.7 2.1 collective-permute-done.11
  52.4 2.0 reshape.138
  54.4 1.9 copy.54
  58.3 4.4 %fusion.2 = (f32[4,4,2,128]{3,2,1,0:T(2,128)S(1)}, f32[4,4,256,128,2]{3,2,4,1,0:T(8,128)}) fusion(pred[4,128,256]{1,2,0:T(8,128)(4,1)S(1)} %compare_and_fusion, bf16[4,128,4,2,64]{4,3,2,1,0:T(2,128)(2,1)} %reshape.140, bf16[4,128,4,64]{1,3,2,0:T(8,128)(2,1)} %copy.55, bf16[4,128,4,64]{1,3,2,0:T(8,128)(2,1)} %copy.54), kind=kOutput, calls=%fused_computation.11 | convolution fusion | flops 138407936 | bytes 5390336 | tf_op jit(solution)/shard_map/nqhgd,nkhd->nhgqk/dot_general | solution.py:56
  68.8 3.3 %fusion.1 = f32[4,4,2,128]{3,2,1,0:T(2,128)S(1)} fusion(f32[4,4,256,128,2]{3,2,4,1,0:T(8,128)} %get-tuple-element.53, f32[4,4,2,128]{3,2,1,0:T(2,128)S(1)} %broadcast_maximum_fusion, pred[4,128,256]{1,2,0:T(8,128)(4,1)S(1)} %copy-done.14), kind=kLoop, calls=%fused_computation.10 | loop fusion | flops 4190208 | bytes 4358144 | tf_op jit(solution)/shard_map/reduce_sum | solution.py:67
  76.7 2.6 collective-permute-done.1
  79.3 2.2 fusion.3
  86.4 22.5 %collective-permute-done.2 = bf16[256,2048]{1,0:T(8,128)(2,1)S(1)} collective-permute-done((bf16[256,2048]{1,0:T(8,128)(2,1)S(1)}, bf16[256,2048]{1,0:T(8,128)(2,1)S(1)}, u32[]{:S(2)}, u32[]{:S(2)}) %collective-permute-start.2) | collective-permute-done | bytes 1048608 | tf_op jit(solution)/shard_map/ppermute | solution.py:77
  108.9 21.8 %collective-permute-done.3 = bf16[256,2048]{1,0:T(8,128)(2,1)S(1)} collective-permute-done((bf16[256,2048]{1,0:T(8,128)(2,1)S(1)}, bf16[256,2048]{1,0:T(8,128)(2,1)S(1)}, u32[]{:S(2)}, u32[]{:S(2)}) %collective-permute-start.3) | collective-permute-done | bytes 1048608 | tf_op jit(solution)/shard_map/ppermute | solution.py:77
  130.8 2.5 pad_maximum_fusion
  138.1 2.6 collective-permute-done.5
  140.7 4.8 %constant_dynamic-update-slice_fusion = bf16[2048,2048]{1,0:T(8,128)(2,1)} fusion(bf16[2048,2048]{1,0:T(8,128)(2,1)} %constant_dynamic-update-slice_fusion.1, bf16[1024,2048]{1,0:T(8,128)(2,1)} %collective-permute-done.5), kind=kLoop, calls=%fused_computation.67 | loop fusion | bytes 8388608 | tf_op jit(solution)/shard_map/concatenate | solution.py:155
  145.5 48.6 %all-gather.4.cloned.1.call-done = bf16[2048,1408]{1,0:T(8,128)(2,1)} async-done(((bf16[512,1408]{1,0:T(8,128)(2,1)}), bf16[2048,1408]{1,0:T(8,128)(2,1)}) %all-gather.4.cloned.1.call-update) | async-done | bytes 5767184 | tf_op jit(solution)/shard_map/all_gather | solution.py:135
  194.1 18.7 %fusion.37 = f32[2048,1408]{0,1:T(8,128)} fusion(bf16[2048,2048]{1,0:T(8,128)(2,1)} %constant_dynamic-update-slice_fusion, bf16[2048,1408]{1,0:T(8,128)(2,1)} %all-gather.4.cloned.1.call-done), kind=kOutput, calls=%fused_computation.108 | convolution fusion | flops 11811160064 | bytes 25690112 | tf_op jit(solution)/shard_map/dot_general | solution.py:157
  212.8 5.3 %fusion = bf16[2048,704]{0,1:T(8,128)(2,1)S(1)} fusion(f32[2048,1408]{0,1:T(8,128)} %fusion.37), kind=kLoop, calls=%fused_computation.1 | loop fusion | flops 8650752 | bytes 14417920 | tf_op jit(solution)/shard_map/convert_element_type | solution.py:159
  218.1 3.7 %convolution_convert_fusion.1 = bf16[2048,1024]{1,0:T(8,128)(2,1)S(1)} fusion(bf16[2048,704]{0,1:T(8,128)(2,1)S(1)} %fusion, bf16[704,1024]{1,0:T(8,128)(2,1)S(1)} %copy_bitcast_fusion.1), kind=kOutput, calls=%fused_computation.9 | convolution fusion | flops 2954887168 | bytes 8519680 | tf_op jit(solution)/shard_map/dot_general | solution.py:163
  224.5 4.2 %all-gather.8.cloned.1.call-done = bf16[8,704,128]{2,1,0:T(8,128)(2,1)} async-done(((bf16[2,704,128]{2,1,0:T(8,128)(2,1)}), bf16[8,704,128]{2,1,0:T(8,128)(2,1)}) %all-gather.8.cloned.1.call-update) | async-done | bytes 1441808 | tf_op jit(solution)/shard_map/all_gather | solution.py:135
  231.0 4.0 %convolution_convert_fusion = bf16[2048,1024]{1,0:T(8,128)(2,1)S(1)} fusion(bf16[2048,704]{0,1:T(8,128)(2,1)S(1)} %copy-done.9, bf16[704,1024]{1,0:T(8,128)(2,1)S(1)} %copy_bitcast_fusion), kind=kOutput, calls=%fused_computation.8 | convolution fusion | flops 2954887168 | bytes 8519680 | tf_op jit(solution)/shard_map/dot_general | solution.py:163
  237.1 2.6 fusion.29
  247.6 7.1 %collective-permute-done.13 = bf16[256,1024]{1,0:T(8,128)(2,1)S(1)} collective-permute-done((bf16[256,1024]{1,0:T(8,128)(2,1)S(1)}, bf16[256,1024]{1,0:T(8,128)(2,1)S(1)}, u32[]{:S(2)}, u32[]{:S(2)}) %collective-permute-start.13) | collective-permute-done | bytes 524320 | tf_op jit(solution)/shard_map/ppermute | solution.py:77
  254.7 2.4 collective-permute-start.19
  257.1 10.3 %collective-permute-done.14 = bf16[256,1024]{1,0:T(8,128)(2,1)S(1)} collective-permute-done((bf16[256,1024]{1,0:T(8,128)(2,1)S(1)}, bf16[256,1024]{1,0:T(8,128)(2,1)S(1)}, u32[]{:S(2)}, u32[]{:S(2)}) %collective-permute-start.14) | collective-permute-done | bytes 524320 | tf_op jit(solution)/shard_map/ppermute | solution.py:77
  267.8 9.5 %collective-permute-done.17 = bf16[256,1024]{1,0:T(8,128)(2,1)S(1)} collective-permute-done((bf16[256,1024]{1,0:T(8,128)(2,1)S(1)}, bf16[256,1024]{1,0:T(8,128)(2,1)S(1)}, u32[]{:S(2)}, u32[]{:S(2)}) %collective-permute-start.17) | collective-permute-done | bytes 524320 | tf_op jit(solution)/shard_map/ppermute | solution.py:77
  277.3 10.5 %collective-permute-done.18 = bf16[256,1024]{1,0:T(8,128)(2,1)S(1)} collective-permute-done((bf16[256,1024]{1,0:T(8,128)(2,1)S(1)}, bf16[256,1024]{1,0:T(8,128)(2,1)S(1)}, u32[]{:S(2)}, u32[]{:S(2)}) %collective-permute-start.18) | collective-permute-done | bytes 524320 | tf_op jit(solution)/shard_map/ppermute | solution.py:77
  289.0 2.6 collective-permute-done.20
  (150 shorter events, 63.7 us)
Async XLA Ops:
  6.5 67.4 %copy-start = (bf16[512,2048]{1,0:T(8,128)(2,1)S(1)}, bf16[512,2048]{1,0:T(8,128)(2,1)}, u32[]{:S(2)}) copy-start(bf16[512,2048]{1,0:T(8,128)(2,1)} %param.17) | copy-start | bytes 6291460
  6.5 130.0 %all-gather.6.cloned.1.call-start = ((), (), s32[]{:S(2)}) async-start(), calls=%async_computation.1 | async-start | bytes 1802240 | tf_op jit(solution)/shard_map/all_gather | solution.py:135
  9.0 13.3 %copy-start.12 = (bf16[2816,128]{1,0:T(8,128)(2,1)S(1)}, bf16[2816,128]{1,0:T(8,128)(2,1)}, u32[]{:S(2)}) copy-start(bf16[2816,128]{1,0:T(8,128)(2,1)} %param.21) | copy-start | bytes 2162692
  13.3 25.6 %collective-permute-start = (bf16[128,640]{1,0:T(8,128)(2,1)}, bf16[128,640]{1,0:T(8,128)(2,1)}, u32[]{:S(2)}, u32[]{:S(2)}) collective-permute-start(bf16[128,640]{1,0:T(8,128)(2,1)} %pad_maximum_fusion.7), channel_id=1, source_target_pairs={{0,2},{2,4},{4,6},{6,8},{8,10},{10,12},{12,14},{14,16},{16,18},{18... | collective-permute-start | bytes 491528 | tf_op jit(solution)/shard_map/ppermute | solution.py:16
  18.8 44.0 %collective-permute-start.6 = (bf16[128,1408]{1,0:T(8,128)(2,1)}, bf16[128,1408]{1,0:T(8,128)(2,1)}, u32[]{:S(2)}, u32[]{:S(2)}) collective-permute-start(bf16[128,1408]{1,0:T(8,128)(2,1)} %pad_maximum_fusion.2), channel_id=1, source_target_pairs={{0,2},{2,0},{4,6},{6,4},{8,10},{10,8},{12,14},{14,12},{16,18},{18,... | collective-permute-start | bytes 1081352 | tf_op jit(solution)/shard_map/ppermute | solution.py:77
  19.7 44.1 %collective-permute-start.7 = (bf16[128,1408]{1,0:T(8,128)(2,1)}, bf16[128,1408]{1,0:T(8,128)(2,1)}, u32[]{:S(2)}, u32[]{:S(2)}) collective-permute-start(bf16[128,1408]{1,0:T(8,128)(2,1)} %pad_maximum_fusion.3), channel_id=1, source_target_pairs={{0,4},{2,6},{4,0},{6,2},{8,12},{10,14},{12,8},{14,10},{16,20},{18,... | collective-permute-start | bytes 1081352 | tf_op jit(solution)/shard_map/ppermute | solution.py:77
  21.2 43.6 %collective-permute-start.8 = (bf16[128,1408]{1,0:T(8,128)(2,1)}, bf16[128,1408]{1,0:T(8,128)(2,1)}, u32[]{:S(2)}, u32[]{:S(2)}) collective-permute-start(bf16[128,1408]{1,0:T(8,128)(2,1)} %pad_maximum_fusion.4), channel_id=1, source_target_pairs={{0,6},{2,4},{4,2},{6,0},{8,14},{10,12},{12,10},{14,8},{16,22},{18,... | collective-permute-start | bytes 1081352 | tf_op jit(solution)/shard_map/ppermute | solution.py:77
  23.1 20.0 %collective-permute-start.9 = (bf16[1,704,128]{2,1,0:T(8,128)(2,1)}, bf16[1,704,128]{2,1,0:T(8,128)(2,1)}, u32[]{:S(2)}, u32[]{:S(2)}) collective-permute-start(bf16[1,704,128]{2,1,0:T(8,128)(2,1)} %get-tuple-element.41), channel_id=1, source_target_pairs={{0,2},{2,0},{4,6},{6,4},{8,10},{10,8},{12,14},{14,12},{16,18},{18,... | collective-permute-start | bytes 540680 | tf_op jit(solution)/shard_map/ppermute | solution.py:77
  25.1 10.1 %copy-start.22 = (f32[8]{0:T(128)S(1)}, f32[8]{0:T(128)}, u32[]{:S(2)}) copy-start(f32[8]{0:T(128)} %param.15) | copy-start | bytes 100
  38.9 8.8 %collective-permute-start.10 = (bf16[1,704,128]{2,1,0:T(8,128)(2,1)}, bf16[1,704,128]{2,1,0:T(8,128)(2,1)S(1)}, u32[]{:S(2)}, u32[]{:S(2)}) collective-permute-start(bf16[1,704,128]{2,1,0:T(8,128)(2,1)} %get-tuple-element.40), channel_id=1, source_target_pairs={{0,4},{2,6},{4,0},{6,2},{8,12},{10,14},{12,8},{14,10},{16,20},{18,... | collective-permute-start | bytes 540680 | tf_op jit(solution)/shard_map/ppermute | solution.py:77
  43.1 6.6 %collective-permute-start.11 = (bf16[1,704,128]{2,1,0:T(8,128)(2,1)}, bf16[1,704,128]{2,1,0:T(8,128)(2,1)S(1)}, u32[]{:S(2)}, u32[]{:S(2)}) collective-permute-start(bf16[1,704,128]{2,1,0:T(8,128)(2,1)} %get-tuple-element.39), channel_id=1, source_target_pairs={{0,6},{2,4},{4,2},{6,0},{8,14},{10,12},{12,10},{14,8},{16,22},{18,... | collective-permute-start | bytes 540680 | tf_op jit(solution)/shard_map/ppermute | solution.py:77
  50.7 143.4 %all-gather.4.cloned.1.call-start = ((), (), s32[]{:S(2)}) async-start(), calls=%async_computation | async-start | bytes 7208960 | tf_op jit(solution)/shard_map/all_gather | solution.py:135
  58.3 4.4 %copy-start.13 = (pred[4,128,256]{1,2,0:T(8,128)(4,1)}, pred[4,128,256]{1,2,0:T(8,128)(4,1)S(1)}, u32[]{:S(2)}) copy-start(pred[4,128,256]{1,2,0:T(8,128)(4,1)S(1)} %compare_and_fusion) | copy-start | bytes 393220
  58.3 4.4 %copy-start.19 = (f32[4,2]{1,0:T(4,128)S(1)}, f32[4,2]{1,0:T(4,128)}, u32[]{:S(2)}) copy-start(f32[4,2]{1,0:T(4,128)} %max.18) | copy-start | bytes 100
  67.0 161.7 %all-gather.8.cloned.1.call-start = ((), (), s32[]{:S(2)}) async-start(), calls=%async_computation.2 | async-start | bytes 1802240 | tf_op jit(solution)/shard_map/all_gather | solution.py:135
  76.6 2.7 collective-permute-start.1
  76.7 4.9 %copy-start.21 = (f32[2048]{0:T(1024)S(1)}, f32[2048]{0:T(1024)}, u32[]{:S(2)}) copy-start(f32[2048]{0:T(1024)} %param.18) | copy-start | bytes 24580
  82.9 26.0 %collective-permute-start.2 = (bf16[256,2048]{1,0:T(8,128)(2,1)S(1)}, bf16[256,2048]{1,0:T(8,128)(2,1)S(1)}, u32[]{:S(2)}, u32[]{:S(2)}) collective-permute-start(bf16[256,2048]{1,0:T(8,128)(2,1)S(1)} %get-tuple-element.24), channel_id=1, source_target_pairs={{0,2},{2,0},{4,6},{6,4},{8,10},{10,8},{12,14},{14,12},{16,18},{18,... | collective-permute-start | bytes 3145736 | tf_op jit(solution)/shard_map/ppermute | solution.py:77
  83.4 47.4 %collective-permute-start.3 = (bf16[256,2048]{1,0:T(8,128)(2,1)S(1)}, bf16[256,2048]{1,0:T(8,128)(2,1)S(1)}, u32[]{:S(2)}, u32[]{:S(2)}) collective-permute-start(bf16[256,2048]{1,0:T(8,128)(2,1)S(1)} %get-tuple-element.24), channel_id=1, source_target_pairs={{0,4},{2,6},{4,0},{6,2},{8,12},{10,14},{12,8},{14,10},{16,20},{18,... | collective-permute-start | bytes 3145736 | tf_op jit(solution)/shard_map/ppermute | solution.py:77
  84.9 45.9 %collective-permute-start.4 = (bf16[256,2048]{1,0:T(8,128)(2,1)S(1)}, bf16[256,2048]{1,0:T(8,128)(2,1)S(1)}, u32[]{:S(2)}, u32[]{:S(2)}) collective-permute-start(bf16[256,2048]{1,0:T(8,128)(2,1)S(1)} %get-tuple-element.24), channel_id=1, source_target_pairs={{0,6},{2,4},{4,2},{6,0},{8,14},{10,12},{12,10},{14,8},{16,22},{18,... | collective-permute-start | bytes 3145736 | tf_op jit(solution)/shard_map/ppermute | solution.py:77
  133.2 7.5 %collective-permute-start.5 = (bf16[1024,2048]{1,0:T(8,128)(2,1)}, bf16[1024,2048]{1,0:T(8,128)(2,1)}, u32[]{:S(2)}, u32[]{:S(2)}) collective-permute-start(bf16[1024,2048]{1,0:T(8,128)(2,1)} %pad_maximum_fusion), channel_id=1, source_target_pairs={{0,1},{1,0},{2,3},{3,2},{4,5},{5,4},{6,7},{7,6},{8,9},{9,8},{10,11... | collective-permute-start | bytes 12582920 | tf_op jit(solution)/shard_map/ppermute | solution.py:77
  218.1 3.7 %copy-start.8 = (bf16[2048,704]{0,1:T(8,128)(2,1)}, bf16[2048,704]{0,1:T(8,128)(2,1)S(1)}, u32[]{:S(2)}) copy-start(bf16[2048,704]{0,1:T(8,128)(2,1)S(1)} %fusion) | copy-start | bytes 8650756
  224.5 10.7 %collective-permute-start.12 = (bf16[1024,1024]{1,0:T(8,128)(2,1)}, bf16[1024,1024]{1,0:T(8,128)(2,1)}, u32[]{:S(2)}, u32[]{:S(2)}) collective-permute-start(bf16[1024,1024]{1,0:T(8,128)(2,1)} %slice.179), channel_id=1, source_target_pairs={{0,1},{1,0},{2,3},{3,2},{4,5},{5,4},{6,7},{7,6},{8,9},{9,8},{10,11... | collective-permute-start | bytes 6291464 | tf_op jit(solution)/shard_map/ppermute | solution.py:77
  235.1 8.3 %collective-permute-start.16 = (bf16[1024,1024]{1,0:T(8,128)(2,1)S(1)}, bf16[1024,1024]{1,0:T(8,128)(2,1)S(1)}, u32[]{:S(2)}, u32[]{:S(2)}) collective-permute-start(bf16[1024,1024]{1,0:T(8,128)(2,1)S(1)} %slice.187), channel_id=1, source_target_pairs={{0,1},{1,0},{2,3},{3,2},{4,5},{5,4},{6,7},{7,6},{8,9},{9,8},{10,11... | collective-permute-start | bytes 6291464 | tf_op jit(solution)/shard_map/ppermute | solution.py:77
  239.9 14.9 %collective-permute-start.13 = (bf16[256,1024]{1,0:T(8,128)(2,1)S(1)}, bf16[256,1024]{1,0:T(8,128)(2,1)S(1)}, u32[]{:S(2)}, u32[]{:S(2)}) collective-permute-start(bf16[256,1024]{1,0:T(8,128)(2,1)S(1)} %get-tuple-element.34), channel_id=1, source_target_pairs={{0,2},{2,0},{4,6},{6,4},{8,10},{10,8},{12,14},{14,12},{16,18},{18,... | collective-permute-start | bytes 1572872 | tf_op jit(solution)/shard_map/ppermute | solution.py:77
  241.4 26.0 %collective-permute-start.14 = (bf16[256,1024]{1,0:T(8,128)(2,1)S(1)}, bf16[256,1024]{1,0:T(8,128)(2,1)S(1)}, u32[]{:S(2)}, u32[]{:S(2)}) collective-permute-start(bf16[256,1024]{1,0:T(8,128)(2,1)S(1)} %get-tuple-element.36), channel_id=1, source_target_pairs={{0,4},{2,6},{4,0},{6,2},{8,12},{10,14},{12,8},{14,10},{16,20},{18,... | collective-permute-start | bytes 1572872 | tf_op jit(solution)/shard_map/ppermute | solution.py:77
  242.9 24.6 %collective-permute-start.15 = (bf16[256,1024]{1,0:T(8,128)(2,1)S(1)}, bf16[256,1024]{1,0:T(8,128)(2,1)S(1)}, u32[]{:S(2)}, u32[]{:S(2)}) collective-permute-start(bf16[256,1024]{1,0:T(8,128)(2,1)S(1)} %get-tuple-element.35), channel_id=1, source_target_pairs={{0,6},{2,4},{4,2},{6,0},{8,14},{10,12},{12,10},{14,8},{16,22},{18,... | collective-permute-start | bytes 1572872 | tf_op jit(solution)/shard_map/ppermute | solution.py:77
  244.6 32.6 %collective-permute-start.17 = (bf16[256,1024]{1,0:T(8,128)(2,1)S(1)}, bf16[256,1024]{1,0:T(8,128)(2,1)S(1)}, u32[]{:S(2)}, u32[]{:S(2)}) collective-permute-start(bf16[256,1024]{1,0:T(8,128)(2,1)S(1)} %get-tuple-element.31), channel_id=1, source_target_pairs={{0,2},{2,0},{4,6},{6,4},{8,10},{10,8},{12,14},{14,12},{16,18},{18,... | collective-permute-start | bytes 1572872 | tf_op jit(solution)/shard_map/ppermute | solution.py:77
  246.2 41.6 %collective-permute-start.18 = (bf16[256,1024]{1,0:T(8,128)(2,1)S(1)}, bf16[256,1024]{1,0:T(8,128)(2,1)S(1)}, u32[]{:S(2)}, u32[]{:S(2)}) collective-permute-start(bf16[256,1024]{1,0:T(8,128)(2,1)S(1)} %get-tuple-element.33), channel_id=1, source_target_pairs={{0,4},{2,6},{4,0},{6,2},{8,12},{10,14},{12,8},{14,10},{16,20},{18,... | collective-permute-start | bytes 1572872 | tf_op jit(solution)/shard_map/ppermute | solution.py:77
  254.7 33.0 %collective-permute-start.19 = (bf16[256,1024]{1,0:T(8,128)(2,1)S(1)}, bf16[256,1024]{1,0:T(8,128)(2,1)S(1)}, u32[]{:S(2)}, u32[]{:S(2)}) collective-permute-start(bf16[256,1024]{1,0:T(8,128)(2,1)S(1)} %get-tuple-element.32), channel_id=1, source_target_pairs={{0,6},{2,4},{4,2},{6,0},{8,14},{10,12},{12,10},{14,8},{16,22},{18,... | collective-permute-start | bytes 1572872 | tf_op jit(solution)/shard_map/ppermute | solution.py:77
  288.5 4.2 %copy-start.1 = (bf16[512,2048]{1,0:T(8,128)(2,1)S(1)}, bf16[512,2048]{1,0:T(8,128)(2,1)}, u32[]{:S(2)}) copy-start(bf16[512,2048]{1,0:T(8,128)(2,1)} %param.17) | copy-start | bytes 6291460
  288.9 2.7 collective-permute-start.20
  (17 other events, 45.3 us)
Sparse Core Ops, SparseCore 0:
  50.8 35.9 all-gather.5
  88.4 105.6 all-gather.3
  195.6 33.0 all-gather.7
where the time goes:
time: 300 us; the launch traced here: 299 us
  waiting for transfers between devices  148 us (49%)
  local copies, waits for them, and re-layouts  49.8 us (17%)
  matrix products  33.3 us (11%)
  other arithmetic  28.7 us (10%)
  starting transfers between devices  25.9 us (9%)
  between operations  13.8 us (5%)
    ppermute x20, waiting for transfers between devices, swap(): return lax.ppermute(shard, axis, [(i, i ^ by) for i in range(size)])  94.9 us
    all_gather x3, waiting for transfers between devices, across(): lax.all_gather(block, 'sp', axis=0, tiled=True, axis_index_groups=columns)  52.8 us
    ppermute x20, starting transfers between devices, swap(): return lax.ppermute(shard, axis, [(i, i ^ by) for i in range(size)])  20.1 us
    dot_general x1, matrix products, on_device(): acts = jnp.dot(tokens, gate_up, preferred_element_type=jnp.float32)  18.7 us
    concatenate x8, local copies, waits for them, and re-layouts, band_rows(): return jnp.concatenate([tensor[:-1], tensor[1:]], axis=1)  12.4 us
    unnamed x56, local copies, waits for them, and re-layouts  9.45 us
    dot_general x2, matrix products, on_device(): jnp.dot(hidden, lax.optimization_barrier(flat(downs[c])), preferred_eleme...  7.68 us
    dynamic_update_slice x9, local copies, waits for them, and re-layouts, in_order(): lax.dynamic_update_slice_in_dim(whole, shard, (place ^ k) * size, axis)  7.09 us
  transfers between devices with their start and end apart: 24, of which 14 were waited for; matrix products, arithmetic and copies ran while one was open for 32% of the time, Pallas kernels for 0%

commit v1 on v0

--- a/solution.py
+++ b/solution.py
@@ -121,8 +121,8 @@
         return piece_of(w_down, seat ^ k, 0, inner)[None]
 
     gate_up_pieces = [gate_up_piece(k) for k in range(inner)]
-    gate_up_pieces, queries, key_rows, values, w_down = lax.optimization_barrier(
-        (gate_up_pieces, queries, key_rows, values, w_down)
+    _, queries, key_rows, values, w_down = lax.optimization_barrier(
+        (gate_up_pieces[1:], queries, key_rows, values, w_down)
     )
     gate_up = in_order(
         gate_up_pieces[0], [swap(gate_up_pieces[k], "sp", k) for k in range(1, inner)], seat, 0
@@ -171,13 +171,19 @@
         for k in range(1, inner):
             sent = swap(sends[k - 1], "sp", k)
             total += sent.astype(jnp.float32)
-        outs.append(total)
-    total = jnp.concatenate(
+        mine = jnp.concatenate(
+            [
+                stream[:, (o * CHUNKS + c) * block : (o * CHUNKS + c + 1) * block]
+                for o in range(outer)
+            ],
+            axis=1,
+        )
+        mine = (mine.astype(jnp.float32) + total).astype(jnp.bfloat16)
+        outs.append(in_order(mine, [swap(mine, "tp", k) for k in range(1, tp)], core, 0))
+    return jnp.concatenate(
         [outs[c][:, o * block : (o + 1) * block] for o in range(outer) for c in range(CHUNKS)],
         axis=1,
     )
-    out = (stream.astype(jnp.float32) + total).astype(jnp.bfloat16)
-    return in_order(out, [swap(out, "tp", k) for k in range(1, tp)], core, 0)
 
 
 def solution(mesh):

time: 300 us -> 299 us (level)
  waiting for transfers between devices: 148 us -> 142 us
    all_gather x3, waiting for transfers between devices: 52.8 us -> 48.6 us  [across(): lax.all_gather(block, 'sp', axis=0, tiled=True, axis_index_groups=columns)]
    another operation x2 -> x0, other arithmetic: 3.67 us -> none
    add x2, other arithmetic: 0.62 us -> 3.67 us  [on_device(): near_sum += swap(mlp_term[k], 'tp', k).astype(jnp.float32)]
    unnamed x56 -> x54, local copies, waits for them, and re-layouts: 9.45 us -> 11.3 us
    ppermute x20 -> x21, waiting for transfers between devices: 94.9 us -> 93.7 us  [swap(): return lax.ppermute(shard, axis, [(i, i ^ by) for i in range(size)])]
    ppermute x20 -> x21, starting transfers between devices: 20.1 us -> 20.7 us  [swap(): return lax.ppermute(shard, axis, [(i, i ^ by) for i in range(size)])]
  transfers between devices with their start and end apart: 24 -> 25, of which waited for: 14 -> 14; matrix products, arithmetic and copies ran while one was open for 32% -> 35% of each run, Pallas kernels for 0% -> 0%
where the time goes in v1:
time: 299 us; the launch traced here: 298 us
  waiting for transfers between devices  142 us (47%)
  local copies, waits for them, and re-layouts  51.6 us (17%)
  matrix products  36.2 us (12%)
  other arithmetic  28.8 us (10%)
  starting transfers between devices  25.5 us (9%)
  between operations  13.8 us (5%)
    ppermute x21, waiting for transfers between devices, swap(): return lax.ppermute(shard, axis, [(i, i ^ by) for i in range(size)])  93.7 us
    all_gather x3, waiting for transfers between devices, across(): lax.all_gather(block, 'sp', axis=0, tiled=True, axis_index_groups=columns)  48.6 us
    ppermute x21, starting transfers between devices, swap(): return lax.ppermute(shard, axis, [(i, i ^ by) for i in range(size)])  20.7 us
    dot_general x1, matrix products, on_device(): acts = jnp.dot(tokens, gate_up, preferred_element_type=jnp.float32)  18.8 us
    concatenate x8, local copies, waits for them, and re-layouts, band_rows(): return jnp.concatenate([tensor[:-1], tensor[1:]], axis=1)  13.1 us
    unnamed x54, local copies, waits for them, and re-layouts  11.3 us
    dot_general x2, matrix products, on_device(): jnp.dot(hidden, lax.optimization_barrier(flat(downs[c])), preferred_eleme...  9.54 us
  transfers between devices with their start and end apart: 25, of which 14 were waited for; matrix products, arithmetic and copies ran while one was open for 35% of the time, Pallas kernels for 0%

profile of v1, /device:TPU:0, one launch (start us, length us, event | category | flops | bytes accessed | tf_op | source)
XLA Modules:
  0.0 298.3 jit_solution(9822653728751220740)
XLA Ops:
  6.6 3.1 %constant_dynamic-slice_fusion = (bf16[128,704]{1,0:T(8,128)(2,1)}, bf16[128,704]{1,0:T(8,128)(2,1)S(1)}, bf16[128,704]{1,0:T(8,128)(2,1)S(1)}, bf16[128,704]{1,...) fusion(bf16[128,2816]{1,0:T(8,128)(2,1)} %param.20, ...), kind=kLoop, calls=%fused_computation.86 | loop fusion | bytes 2883600 | tf_op jit(solution)/shard_map/dynamic_slice | solution.py:82
  10.6 3.0 collective-permute-start.6
  17.7 4.5 %collective-permute-start = (bf16[128,640]{1,0:T(8,128)(2,1)}, bf16[128,640]{1,0:T(8,128)(2,1)}, u32[]{:S(2)}, u32[]{:S(2)}) collective-permute-start(bf16[128,640]{1,0:T(8,128)(2,1)} %pad_maximum_fusion.6), channel_id=1, source_target_pairs={{0,2},{2,4},{4,6},{6,8},{8,10},{10,12},{12,14},{14,16},{16,18},{18... | collective-permute-start | bytes 491528 | tf_op jit(solution)/shard_map/ppermute | solution.py:16
  25.8 2.0 reshape.139
  27.8 2.0 reshape.137
  29.8 3.5 %reshape.140 = bf16[4,128,4,2,64]{4,3,2,1,0:T(2,128)(2,1)} reshape(bf16[512,512]{1,0:T(8,128)(2,1)} %param.11) | data formatting | bytes 1048576 | tf_op jit(solution)/shard_map/reshape | solution.py:55
  44.1 3.6 %collective-permute-done.10 = bf16[1,704,128]{2,1,0:T(8,128)(2,1)S(1)} collective-permute-done((bf16[1,704,128]{2,1,0:T(8,128)(2,1)}, bf16[1,704,128]{2,1,0:T(8,128)(2,1)S(1)}, u32[]{:S(2)}, u32[]{:S(2)}) %collective-permute-start.10) | collective-permute-done | bytes 180256 | tf_op jit(solution)/shard_map/ppermute | solution.py:77
  51.3 2.0 reshape.138
  53.3 2.0 copy.54
  57.2 4.4 %fusion.2 = (f32[4,4,2,128]{3,2,1,0:T(2,128)S(1)}, f32[4,4,256,128,2]{3,2,4,1,0:T(8,128)}) fusion(pred[4,128,256]{1,2,0:T(8,128)(4,1)S(1)} %compare_and_fusion, bf16[4,128,4,2,64]{4,3,2,1,0:T(2,128)(2,1)} %reshape.140, bf16[4,128,4,64]{1,3,2,0:T(8,128)(2,1)} %copy.55, bf16[4,128,4,64]{1,3,2,0:T(8,128)(2,1)} %copy.54), kind=kOutput, calls=%fused_computation.11 | convolution fusion | flops 138407936 | bytes 5390336 | tf_op jit(solution)/shard_map/nqhgd,nkhd->nhgqk/dot_general | solution.py:56
  68.3 3.3 %fusion.1 = f32[4,4,2,128]{3,2,1,0:T(2,128)S(1)} fusion(f32[4,4,256,128,2]{3,2,4,1,0:T(8,128)} %get-tuple-element.55, f32[4,4,2,128]{3,2,1,0:T(2,128)S(1)} %broadcast_maximum_fusion, pred[4,128,256]{1,2,0:T(8,128)(4,1)} %copy-done.11), kind=kLoop, calls=%fused_computation.10 | loop fusion | flops 4190208 | bytes 4358144 | tf_op jit(solution)/shard_map/reduce_sum | solution.py:67
  71.8 2.1 fusion.8
  77.2 2.6 collective-permute-done.1
  79.8 2.2 fusion.3
  86.9 22.5 %collective-permute-done.2 = bf16[256,2048]{1,0:T(8,128)(2,1)S(1)} collective-permute-done((bf16[256,2048]{1,0:T(8,128)(2,1)S(1)}, bf16[256,2048]{1,0:T(8,128)(2,1)S(1)}, u32[]{:S(2)}, u32[]{:S(2)}) %collective-permute-start.2) | collective-permute-done | bytes 1048608 | tf_op jit(solution)/shard_map/ppermute | solution.py:77
  110.3 21.7 %collective-permute-done.4 = bf16[256,2048]{1,0:T(8,128)(2,1)S(1)} collective-permute-done((bf16[256,2048]{1,0:T(8,128)(2,1)S(1)}, bf16[256,2048]{1,0:T(8,128)(2,1)S(1)}, u32[]{:S(2)}, u32[]{:S(2)}) %collective-permute-start.4) | collective-permute-done | bytes 1048608 | tf_op jit(solution)/shard_map/ppermute | solution.py:77
  132.0 2.5 pad_maximum_fusion
  139.3 2.6 collective-permute-done.5
  141.9 4.7 %constant_dynamic-update-slice_fusion = bf16[2048,2048]{1,0:T(8,128)(2,1)} fusion(bf16[2048,2048]{1,0:T(8,128)(2,1)} %constant_dynamic-update-slice_fusion.1, bf16[1024,2048]{1,0:T(8,128)(2,1)} %collective-permute-done.5), kind=kLoop, calls=%fused_computation.69 | loop fusion | bytes 8388608 | tf_op jit(solution)/shard_map/concatenate | solution.py:155
  146.7 45.4 %all-gather.4.cloned.1.call-done = bf16[2048,1408]{1,0:T(8,128)(2,1)} async-done(((bf16[512,1408]{1,0:T(8,128)(2,1)}), bf16[2048,1408]{1,0:T(8,128)(2,1)}) %all-gather.4.cloned.1.call-update) | async-done | bytes 5767184 | tf_op jit(solution)/shard_map/all_gather | solution.py:135
  192.0 18.8 %fusion.42 = f32[2048,1408]{0,1:T(8,128)} fusion(bf16[2048,2048]{1,0:T(8,128)(2,1)} %constant_dynamic-update-slice_fusion, bf16[2048,1408]{1,0:T(8,128)(2,1)} %all-gather.4.cloned.1.call-done), kind=kOutput, calls=%fused_computation.112 | convolution fusion | flops 11811160064 | bytes 25690112 | tf_op jit(solution)/shard_map/dot_general | solution.py:157
  210.9 5.3 %fusion = bf16[2048,704]{0,1:T(8,128)(2,1)S(1)} fusion(f32[2048,1408]{0,1:T(8,128)} %fusion.42), kind=kLoop, calls=%fused_computation.1 | loop fusion | flops 8650752 | bytes 14417920 | tf_op jit(solution)/shard_map/convert_element_type | solution.py:159
  216.2 3.7 %convolution_convert_fusion.1 = bf16[2048,1024]{1,0:T(8,128)(2,1)S(1)} fusion(bf16[2048,704]{0,1:T(8,128)(2,1)S(1)} %fusion, bf16[704,1024]{1,0:T(8,128)(2,1)S(1)} %copy_bitcast_fusion.1), kind=kOutput, calls=%fused_computation.9 | convolution fusion | flops 2954887168 | bytes 8519680 | tf_op jit(solution)/shard_map/dot_general | solution.py:163
  219.9 2.0 copy-done.3
  223.4 3.3 %all-gather.8.cloned.1.call-done = bf16[8,704,128]{2,1,0:T(8,128)(2,1)} async-done(((bf16[2,704,128]{2,1,0:T(8,128)(2,1)}), bf16[8,704,128]{2,1,0:T(8,128)(2,1)}) %all-gather.8.cloned.1.call-update) | async-done | bytes 1441808 | tf_op jit(solution)/shard_map/all_gather | solution.py:135
  228.2 5.8 %convolution_convert_fusion = bf16[2048,1024]{1,0:T(8,128)(2,1)S(1)} fusion(bf16[2048,704]{0,1:T(8,128)(2,1)} %copy-done.8, bf16[704,1024]{1,0:T(8,128)(2,1)S(1)} %copy_bitcast_fusion), kind=kOutput, calls=%fused_computation.8 | convolution fusion | flops 2954887168 | bytes 8519680 | tf_op jit(solution)/shard_map/dot_general | solution.py:163
  236.2 2.6 convert_add_fusion.1
  246.7 7.1 %collective-permute-done.13 = bf16[256,1024]{1,0:T(8,128)(2,1)S(1)} collective-permute-done((bf16[256,1024]{1,0:T(8,128)(2,1)S(1)}, bf16[256,1024]{1,0:T(8,128)(2,1)S(1)}, u32[]{:S(2)}, u32[]{:S(2)}) %collective-permute-start.13) | collective-permute-done | bytes 524320 | tf_op jit(solution)/shard_map/ppermute | solution.py:77
  253.9 2.4 collective-permute-start.20
  256.3 10.3 %collective-permute-done.14 = bf16[256,1024]{1,0:T(8,128)(2,1)S(1)} collective-permute-done((bf16[256,1024]{1,0:T(8,128)(2,1)S(1)}, bf16[256,1024]{1,0:T(8,128)(2,1)S(1)}, u32[]{:S(2)}, u32[]{:S(2)}) %collective-permute-start.14) | collective-permute-done | bytes 524320 | tf_op jit(solution)/shard_map/ppermute | solution.py:77
  267.2 9.2 %collective-permute-done.18 = bf16[256,1024]{1,0:T(8,128)(2,1)S(1)} collective-permute-done((bf16[256,1024]{1,0:T(8,128)(2,1)S(1)}, bf16[256,1024]{1,0:T(8,128)(2,1)S(1)}, u32[]{:S(2)}, u32[]{:S(2)}) %collective-permute-start.18) | collective-permute-done | bytes 524320 | tf_op jit(solution)/shard_map/ppermute | solution.py:77
  276.4 10.4 %collective-permute-done.19 = bf16[256,1024]{1,0:T(8,128)(2,1)S(1)} collective-permute-done((bf16[256,1024]{1,0:T(8,128)(2,1)S(1)}, bf16[256,1024]{1,0:T(8,128)(2,1)S(1)}, u32[]{:S(2)}, u32[]{:S(2)}) %collective-permute-start.19) | collective-permute-done | bytes 524320 | tf_op jit(solution)/shard_map/ppermute | solution.py:77
  (151 shorter events, 63.8 us)
Async XLA Ops:
  6.5 67.9 %copy-start = (bf16[512,2048]{1,0:T(8,128)(2,1)S(1)}, bf16[512,2048]{1,0:T(8,128)(2,1)}, u32[]{:S(2)}) copy-start(bf16[512,2048]{1,0:T(8,128)(2,1)} %param.17) | copy-start | bytes 6291460
  6.5 10.3 %copy-start.17 = (s32[512]{0:T(512)S(1)}, s32[512]{0:T(512)}, u32[]{:S(2)}) copy-start(s32[512]{0:T(512)} %param.14) | copy-start | bytes 6148
  6.5 131.2 %all-gather.6.cloned.1.call-start = ((), (), s32[]{:S(2)}) async-start(), calls=%async_computation.1 | async-start | bytes 1802240 | tf_op jit(solution)/shard_map/all_gather | solution.py:135
  6.5 10.4 %slice-start = ((bf16[512,256]{1,0:T(8,128)(2,1)}), bf16[128,256]{1,0:T(8,128)(2,1)S(1)}, s32[]{:S(2)}) async-start(bf16[512,256]{1,0:T(8,128)(2,1)} %param.12), calls=%async_computation.3 | async-start | bytes 131072 | tf_op jit(solution)/shard_map/slice | solution.py:39
  6.5 10.4 %slice-start.1 = ((bf16[512,256]{1,0:T(8,128)(2,1)}), bf16[128,256]{1,0:T(8,128)(2,1)S(1)}, s32[]{:S(2)}) async-start(bf16[512,256]{1,0:T(8,128)(2,1)} %param.13), calls=%async_computation.4 | async-start | bytes 131072 | tf_op jit(solution)/shard_map/slice | solution.py:40
  6.6 15.6 %copy-start.10 = (bf16[2816,128]{1,0:T(8,128)(2,1)S(1)}, bf16[2816,128]{1,0:T(8,128)(2,1)}, u32[]{:S(2)}) copy-start(bf16[2816,128]{1,0:T(8,128)(2,1)} %param.21) | copy-start | bytes 2162692
  10.6 51.0 %collective-permute-start.6 = (bf16[128,1408]{1,0:T(8,128)(2,1)}, bf16[128,1408]{1,0:T(8,128)(2,1)}, u32[]{:S(2)}, u32[]{:S(2)}) collective-permute-start(bf16[128,1408]{1,0:T(8,128)(2,1)} %pad_maximum_fusion.1), channel_id=1, source_target_pairs={{0,2},{2,0},{4,6},{6,4},{8,10},{10,8},{12,14},{14,12},{16,18},{18,... | collective-permute-start | bytes 1081352 | tf_op jit(solution)/shard_map/ppermute | solution.py:77
  14.5 48.2 %collective-permute-start.7 = (bf16[128,1408]{1,0:T(8,128)(2,1)}, bf16[128,1408]{1,0:T(8,128)(2,1)}, u32[]{:S(2)}, u32[]{:S(2)}) collective-permute-start(bf16[128,1408]{1,0:T(8,128)(2,1)} %pad_maximum_fusion.2), channel_id=1, source_target_pairs={{0,4},{2,6},{4,0},{6,2},{8,12},{10,14},{12,8},{14,10},{16,20},{18,... | collective-permute-start | bytes 1081352 | tf_op jit(solution)/shard_map/ppermute | solution.py:77
  16.9 46.8 %collective-permute-start.8 = (bf16[128,1408]{1,0:T(8,128)(2,1)}, bf16[128,1408]{1,0:T(8,128)(2,1)}, u32[]{:S(2)}, u32[]{:S(2)}) collective-permute-start(bf16[128,1408]{1,0:T(8,128)(2,1)} %pad_maximum_fusion.3), channel_id=1, source_target_pairs={{0,6},{2,4},{4,2},{6,0},{8,14},{10,12},{12,10},{14,8},{16,22},{18,... | collective-permute-start | bytes 1081352 | tf_op jit(solution)/shard_map/ppermute | solution.py:77
  17.7 21.2 %collective-permute-start = (bf16[128,640]{1,0:T(8,128)(2,1)}, bf16[128,640]{1,0:T(8,128)(2,1)}, u32[]{:S(2)}, u32[]{:S(2)}) collective-permute-start(bf16[128,640]{1,0:T(8,128)(2,1)} %pad_maximum_fusion.6), channel_id=1, source_target_pairs={{0,2},{2,4},{4,6},{6,8},{8,10},{10,12},{12,14},{14,16},{16,18},{18... | collective-permute-start | bytes 491528 | tf_op jit(solution)/shard_map/ppermute | solution.py:16
  23.0 19.0 %collective-permute-start.9 = (bf16[1,704,128]{2,1,0:T(8,128)(2,1)}, bf16[1,704,128]{2,1,0:T(8,128)(2,1)}, u32[]{:S(2)}, u32[]{:S(2)}) collective-permute-start(bf16[1,704,128]{2,1,0:T(8,128)(2,1)} %get-tuple-element.43), channel_id=1, source_target_pairs={{0,2},{2,0},{4,6},{6,4},{8,10},{10,8},{12,14},{14,12},{16,18},{18,... | collective-permute-start | bytes 540680 | tf_op jit(solution)/shard_map/ppermute | solution.py:77
  23.8 11.4 %copy-start.21 = (f32[8]{0:T(128)S(1)}, f32[8]{0:T(128)}, u32[]{:S(2)}) copy-start(f32[8]{0:T(128)} %param.15) | copy-start | bytes 100
  38.9 8.8 %collective-permute-start.10 = (bf16[1,704,128]{2,1,0:T(8,128)(2,1)}, bf16[1,704,128]{2,1,0:T(8,128)(2,1)S(1)}, u32[]{:S(2)}, u32[]{:S(2)}) collective-permute-start(bf16[1,704,128]{2,1,0:T(8,128)(2,1)} %get-tuple-element.42), channel_id=1, source_target_pairs={{0,4},{2,6},{4,0},{6,2},{8,12},{10,14},{12,8},{14,10},{16,20},{18,... | collective-permute-start | bytes 540680 | tf_op jit(solution)/shard_map/ppermute | solution.py:77
  42.0 6.6 %collective-permute-start.11 = (bf16[1,704,128]{2,1,0:T(8,128)(2,1)}, bf16[1,704,128]{2,1,0:T(8,128)(2,1)S(1)}, u32[]{:S(2)}, u32[]{:S(2)}) collective-permute-start(bf16[1,704,128]{2,1,0:T(8,128)(2,1)} %get-tuple-element.41), channel_id=1, source_target_pairs={{0,6},{2,4},{4,2},{6,0},{8,14},{10,12},{12,10},{14,8},{16,22},{18,... | collective-permute-start | bytes 540680 | tf_op jit(solution)/shard_map/ppermute | solution.py:77
  49.6 142.4 %all-gather.4.cloned.1.call-start = ((), (), s32[]{:S(2)}) async-start(), calls=%async_computation | async-start | bytes 7208960 | tf_op jit(solution)/shard_map/all_gather | solution.py:135
  65.9 160.8 %all-gather.8.cloned.1.call-start = ((), (), s32[]{:S(2)}) async-start(), calls=%async_computation.2 | async-start | bytes 1802240 | tf_op jit(solution)/shard_map/all_gather | solution.py:135
  77.0 5.0 %copy-start.20 = (f32[2048]{0:T(1024)S(1)}, f32[2048]{0:T(1024)}, u32[]{:S(2)}) copy-start(f32[2048]{0:T(1024)} %param.18) | copy-start | bytes 24580
  77.1 2.7 collective-permute-start.1
  83.4 26.0 %collective-permute-start.2 = (bf16[256,2048]{1,0:T(8,128)(2,1)S(1)}, bf16[256,2048]{1,0:T(8,128)(2,1)S(1)}, u32[]{:S(2)}, u32[]{:S(2)}) collective-permute-start(bf16[256,2048]{1,0:T(8,128)(2,1)S(1)} %get-tuple-element.18), channel_id=1, source_target_pairs={{0,2},{2,0},{4,6},{6,4},{8,10},{10,8},{12,14},{14,12},{16,18},{18,... | collective-permute-start | bytes 3145736 | tf_op jit(solution)/shard_map/ppermute | solution.py:77
  84.5 25.7 %collective-permute-start.3 = (bf16[256,2048]{1,0:T(8,128)(2,1)S(1)}, bf16[256,2048]{1,0:T(8,128)(2,1)S(1)}, u32[]{:S(2)}, u32[]{:S(2)}) collective-permute-start(bf16[256,2048]{1,0:T(8,128)(2,1)S(1)} %get-tuple-element.18), channel_id=1, source_target_pairs={{0,4},{2,6},{4,0},{6,2},{8,12},{10,14},{12,8},{14,10},{16,20},{18,... | collective-permute-start | bytes 3145736 | tf_op jit(solution)/shard_map/ppermute | solution.py:77
  85.4 46.6 %collective-permute-start.4 = (bf16[256,2048]{1,0:T(8,128)(2,1)S(1)}, bf16[256,2048]{1,0:T(8,128)(2,1)S(1)}, u32[]{:S(2)}, u32[]{:S(2)}) collective-permute-start(bf16[256,2048]{1,0:T(8,128)(2,1)S(1)} %get-tuple-element.18), channel_id=1, source_target_pairs={{0,6},{2,4},{4,2},{6,0},{8,14},{10,12},{12,10},{14,8},{16,22},{18,... | collective-permute-start | bytes 3145736 | tf_op jit(solution)/shard_map/ppermute | solution.py:77
  134.4 7.5 %collective-permute-start.5 = (bf16[1024,2048]{1,0:T(8,128)(2,1)}, bf16[1024,2048]{1,0:T(8,128)(2,1)}, u32[]{:S(2)}, u32[]{:S(2)}) collective-permute-start(bf16[1024,2048]{1,0:T(8,128)(2,1)} %pad_maximum_fusion), channel_id=1, source_target_pairs={{0,1},{1,0},{2,3},{3,2},{4,5},{5,4},{6,7},{7,6},{8,9},{9,8},{10,11... | collective-permute-start | bytes 12582920 | tf_op jit(solution)/shard_map/ppermute | solution.py:77
  223.4 10.9 %collective-permute-start.12 = (bf16[1024,1024]{1,0:T(8,128)(2,1)}, bf16[1024,1024]{1,0:T(8,128)(2,1)}, u32[]{:S(2)}, u32[]{:S(2)}) collective-permute-start(bf16[1024,1024]{1,0:T(8,128)(2,1)} %slice.215), channel_id=1, source_target_pairs={{0,1},{1,0},{2,3},{3,2},{4,5},{5,4},{6,7},{7,6},{8,9},{9,8},{10,11... | collective-permute-start | bytes 6291464 | tf_op jit(solution)/shard_map/ppermute | solution.py:77
  234.2 8.3 %collective-permute-start.17 = (bf16[1024,1024]{1,0:T(8,128)(2,1)S(1)}, bf16[1024,1024]{1,0:T(8,128)(2,1)S(1)}, u32[]{:S(2)}, u32[]{:S(2)}) collective-permute-start(bf16[1024,1024]{1,0:T(8,128)(2,1)S(1)} %slice.227), channel_id=1, source_target_pairs={{0,1},{1,0},{2,3},{3,2},{4,5},{5,4},{6,7},{7,6},{8,9},{9,8},{10,11... | collective-permute-start | bytes 6291464 | tf_op jit(solution)/shard_map/ppermute | solution.py:77
  239.0 14.9 %collective-permute-start.13 = (bf16[256,1024]{1,0:T(8,128)(2,1)S(1)}, bf16[256,1024]{1,0:T(8,128)(2,1)S(1)}, u32[]{:S(2)}, u32[]{:S(2)}) collective-permute-start(bf16[256,1024]{1,0:T(8,128)(2,1)S(1)} %get-tuple-element.28), channel_id=1, source_target_pairs={{0,2},{2,0},{4,6},{6,4},{8,10},{10,8},{12,14},{14,12},{16,18},{18,... | collective-permute-start | bytes 1572872 | tf_op jit(solution)/shard_map/ppermute | solution.py:77
  240.5 26.0 %collective-permute-start.14 = (bf16[256,1024]{1,0:T(8,128)(2,1)S(1)}, bf16[256,1024]{1,0:T(8,128)(2,1)S(1)}, u32[]{:S(2)}, u32[]{:S(2)}) collective-permute-start(bf16[256,1024]{1,0:T(8,128)(2,1)S(1)} %get-tuple-element.30), channel_id=1, source_target_pairs={{0,4},{2,6},{4,0},{6,2},{8,12},{10,14},{12,8},{14,10},{16,20},{18,... | collective-permute-start | bytes 1572872 | tf_op jit(solution)/shard_map/ppermute | solution.py:77
  242.0 24.6 %collective-permute-start.15 = (bf16[256,1024]{1,0:T(8,128)(2,1)S(1)}, bf16[256,1024]{1,0:T(8,128)(2,1)S(1)}, u32[]{:S(2)}, u32[]{:S(2)}) collective-permute-start(bf16[256,1024]{1,0:T(8,128)(2,1)S(1)} %get-tuple-element.29), channel_id=1, source_target_pairs={{0,6},{2,4},{4,2},{6,0},{8,14},{10,12},{12,10},{14,8},{16,22},{18,... | collective-permute-start | bytes 1572872 | tf_op jit(solution)/shard_map/ppermute | solution.py:77
  243.7 32.6 %collective-permute-start.18 = (bf16[256,1024]{1,0:T(8,128)(2,1)S(1)}, bf16[256,1024]{1,0:T(8,128)(2,1)S(1)}, u32[]{:S(2)}, u32[]{:S(2)}) collective-permute-start(bf16[256,1024]{1,0:T(8,128)(2,1)S(1)} %get-tuple-element.25), channel_id=1, source_target_pairs={{0,2},{2,0},{4,6},{6,4},{8,10},{10,8},{12,14},{14,12},{16,18},{18,... | collective-permute-start | bytes 1572872 | tf_op jit(solution)/shard_map/ppermute | solution.py:77
  245.3 41.6 %collective-permute-start.19 = (bf16[256,1024]{1,0:T(8,128)(2,1)S(1)}, bf16[256,1024]{1,0:T(8,128)(2,1)S(1)}, u32[]{:S(2)}, u32[]{:S(2)}) collective-permute-start(bf16[256,1024]{1,0:T(8,128)(2,1)S(1)} %get-tuple-element.27), channel_id=1, source_target_pairs={{0,4},{2,6},{4,0},{6,2},{8,12},{10,14},{12,8},{14,10},{16,20},{18,... | collective-permute-start | bytes 1572872 | tf_op jit(solution)/shard_map/ppermute | solution.py:77
  253.9 33.0 %collective-permute-start.20 = (bf16[256,1024]{1,0:T(8,128)(2,1)S(1)}, bf16[256,1024]{1,0:T(8,128)(2,1)S(1)}, u32[]{:S(2)}, u32[]{:S(2)}) collective-permute-start(bf16[256,1024]{1,0:T(8,128)(2,1)S(1)} %get-tuple-element.26), channel_id=1, source_target_pairs={{0,6},{2,4},{4,2},{6,0},{8,14},{10,12},{12,10},{14,8},{16,22},{18,... | collective-permute-start | bytes 1572872 | tf_op jit(solution)/shard_map/ppermute | solution.py:77
  267.1 20.4 %collective-permute-start.16 = (bf16[256,1024]{1,0:T(8,128)(2,1)S(1)}, bf16[256,1024]{1,0:T(8,128)(2,1)S(1)}, u32[]{:S(2)}, u32[]{:S(2)}) collective-permute-start(bf16[256,1024]{1,0:T(8,128)(2,1)S(1)} %get-tuple-element.16), channel_id=1, source_target_pairs={{0,1},{1,0},{2,3},{3,2},{4,5},{5,4},{6,7},{7,6},{8,9},{9,8},{10,11... | collective-permute-start | bytes 1572872 | tf_op jit(solution)/shard_map/ppermute | solution.py:77
  287.4 2.0 collective-permute-start.21
  (17 other events, 52.9 us)
Sparse Core Ops, SparseCore 0:
  49.7 35.0 all-gather.5
  86.3 105.6 all-gather.3
  193.6 33.0 all-gather.7
